TPU v7x, 256 devices: a 4x2x16 block of a 4x16x16 slice. The times are simulated.
256 devices in a mesh: grp: 2 (over y), sp: 16 (over z), dp: 8 (over x, core).
Axes of the slice: x: 4, y: 2, z: 16, core: 2. Of those that a mesh axis runs over, the one named last changes fastest.
The devices are a block of a 4x16x16 slice.
Arguments:
- activations: bfloat16 [16, 8192, 2048], P(('grp', 'dp'), 'sp'), parts along dimension 0, may hold values from -6 to 6
- value_weight: bfloat16 [2048, 1024], P('sp', 'dp'), may hold values from -0.125 to 0.125
- gate_weight: bfloat16 [2048, 1024], P('sp', 'dp'), may hold values from -0.125 to 0.125
- conv_taps: float32 [31, 1024], replicated, may hold values from -4 to 4
- conv_bias: float32 [1024], replicated, may hold values from -3 to 3
- norm_gain: float32 [1024], replicated, may hold values from 0.1 to 1.9
- norm_bias: float32 [1024], replicated, may hold values from -3 to 3
- out_weight: bfloat16 [1024, 2048], P('sp', 'dp'), may hold values from -0.1875 to 0.1875
Outputs:
- mixed_out: bfloat16 [16, 8192, 2048], P(('grp', 'dp'), 'sp'), parts along dimension 0
There are 2 independent parts, one for each index of `grp`. A program takes and returns all parts, laid end to end along the dimension named above; an argument that names none is the same for every part. Nothing has to cross between parts.
All inputs are finite; a program needn't handle non-finite values.
Results may differ from a plain program's by a relative error of at most 0.013.
Values may be sent and summed in bfloat16 or wider, within the bound.
No kernel may reach another device: no remote copies, remote signals or barrier semaphores. Data moves between devices by JAX's collectives and lax.ppermute only.
A program may use at most 64 MiB of HBM per device.

v0:
```python
import jax
import jax.numpy as jnp
from jax import lax
from jax.sharding import PartitionSpec as P

epsilon = 1e-05


def in_one_piece(arrays, axis, dim, along):
    widths = [a.shape[along] for a in arrays]
    both = jnp.concatenate(arrays, axis=along)
    filled = lax.all_gather(both, axis, axis=dim, tiled=True)
    return tuple(jnp.split(filled, [sum(widths[:k]) for k in range(1, len(widths))], axis=along))


def passed_along(value, axis, steps):
    count = lax.axis_size(axis)
    first, last = (max(0, -steps), min(count, count - steps))
    return lax.ppermute(value, axis, [(source, source + steps) for source in range(first, last)])


def local(
    activations, value_weight, gate_weight, conv_taps, conv_bias, norm_gain, norm_bias, out_weight
):
    tokens = activations[0]
    tok_rows = tokens.shape[0]
    kernel_len = conv_taps.shape[0]
    whole_value, whole_gate = in_one_piece((value_weight, gate_weight), "sp", 0, 1)
    stacked = jnp.stack([whole_value, whole_gate], axis=0)
    both_rows = jnp.einsum(
        "td,kdc->ktc",
        tokens,
        lax.all_gather(stacked, "dp", axis=2, tiled=True),
        preferred_element_type=jnp.float32,
    )
    value_rows = both_rows[0]
    gate_rows = both_rows[1]
    value_half = value_rows.astype(jnp.bfloat16)
    gate_half = gate_rows.astype(jnp.bfloat16)
    gated_rows = (
        value_half.astype(jnp.float32) * jax.nn.sigmoid(gate_half.astype(jnp.float32))
    ).astype(jnp.bfloat16)
    prior = passed_along(gated_rows[tok_rows - (kernel_len - 1) :], "sp", 1)
    padded = jnp.concatenate([prior, gated_rows], axis=0).astype(jnp.float32)
    conv_sum = jnp.zeros(gated_rows.shape, jnp.float32) + conv_bias[None, :]
    for tap_index in range(kernel_len):
        conv_sum = (
            conv_sum + conv_taps[tap_index][None, :] * padded[tap_index : tap_index + tok_rows]
        )
    mean_row = jnp.mean(conv_sum, axis=-1, keepdims=True)
    centered = conv_sum - mean_row
    spread = jnp.mean(centered * centered, axis=-1, keepdims=True)
    normed = centered * lax.rsqrt(spread + epsilon) * norm_gain[None, :] + norm_bias[None, :]
    swished = jax.nn.silu(normed).astype(jnp.bfloat16)
    whole_output = lax.all_gather(out_weight, "sp", axis=0, tiled=True)
    result = jnp.dot(
        swished,
        lax.all_gather(whole_output, "dp", axis=1, tiled=True),
        preferred_element_type=jnp.float32,
    )
    return result.astype(jnp.bfloat16)[None]


def solution(mesh):
    in_specs = (
        P(("grp", "dp"), "sp", None),
        P("sp", "dp"),
        P("sp", "dp"),
        P(),
        P(),
        P(),
        P(),
        P("sp", "dp"),
    )
    out_specs = P(("grp", "dp"), "sp", None)
    return jax.shard_map(local, mesh=mesh, in_specs=in_specs, out_specs=out_specs, check_vma=False)
```

profile of v0, /device:TPU:33, one launch (start us, length us, event | category | flops | bytes accessed | tf_op | source)
XLA Modules:
  0.0 210.3 jit_solution(13872795906434215468)
XLA Ops:
  6.5 0.0 copy-start
  6.6 0.0 all-gather.4.cloned.1.call-start
  6.6 1.6 pad_maximum_fusion.1
  8.1 0.1 all-gather.4.cloned.1.call-update
  8.2 0.1 all-gather.6.cloned.1.call-start
  8.2 73.8 %all-gather.4.cloned.1.call-done = bf16[2048,256]{1,0:T(8,128)(2,1)} async-done(((bf16[128,256]{1,0:T(8,128)(2,1)}), bf16[2048,256]{1,0:T(8,128)(2,1)}) %all-gather.4.cloned.1.call-update) | async-done | bytes 1048592 | tf_op jit(solution)/shard_map/all_gather | solution.py:12
  82.0 1.3 slice_bitcast_fusion.1
  83.3 0.0 copy-start.3
  83.3 0.0 copy-start.2
  83.3 1.1 pad_maximum_fusion
  84.4 0.1 all-gather.6.cloned.1.call-update
  84.4 0.1 all-gather.8.cloned.1.call-start
  84.5 0.0 copy-done.3
  84.5 26.9 %all_gather.14 = bf16[1024,256]{1,0:T(8,128)(2,1)} all-gather(bf16[64,256]{1,0:T(8,128)(2,1)S(1)} %copy-done.3), channel_id=1, replica_groups=mesh['grp'=2,'sp'=16,'dp'=8] {'sp'}, dimensions={0}, use_global_device_ids=true | all-gather | bytes 557056 | tf_op jit(solution)/shard_map/all_gather | solution.py:55
  111.4 0.1 all-gather.8.cloned.1.call-update
  111.5 0.0 copy-done.2
  111.5 0.1 fusion.44
  111.6 40.7 %all-gather.6.cloned.1.call-done = bf16[2,2048,1024]{2,1,0:T(8,128)(2,1)} async-done(((bf16[2,2048,128]{2,1,0:T(8,128)(2,1)}), bf16[2,2048,1024]{2,1,0:T(8,128)(2,1)}) %all-gather.6.cloned.1.call-update) | async-done | bytes 8388624 | tf_op jit(solution)/shard_map/all_gather | solution.py:33
  152.4 8.1 %convert_bitcast_fusion = bf16[2,512,1024]{2,1,0:T(8,128)(2,1)S(1)} fusion(bf16[2,2048,1024]{2,1,0:T(8,128)(2,1)} %all-gather.6.cloned.1.call-done, bf16[1,512,2048]{2,1,0:T(8,128)(2,1)S(1)} %copy-done), kind=kOutput, calls=%fused_computation.67 | convolution fusion | flops 4296015872 | bytes 12582912 | tf_op jit(solution)/shard_map/td,kdc->ktc/dot_general | solution.py:30
  160.4 0.6 multiply_convert_fusion
  161.1 3.2 %collective-permute-start = (bf16[30,1024]{1,0:T(8,128)(2,1)S(1)}, bf16[30,1024]{1,0:T(8,128)(2,1)S(1)}, u32[]{:S(2)}, u32[]{:S(2)}) collective-permute-start(bf16[30,1024]{1,0:T(8,128)(2,1)S(1)} %slice_bitcast_fusion.2), channel_id=1, source_target_pairs={{0,8},{8,16},{16,24},{24,32},{32,40},{40,48},{48,56},{56,64},{64,7... | collective-permute-start | bytes 184328 | tf_op jit(solution)/shard_map/ppermute | solution.py:19
  164.3 0.6 fusion.48
  164.9 0.0 copy-start.4
  164.9 0.7 collective-permute-done
  165.6 0.3 maximum_convert_fusion
  165.9 9.8 %fusion.42 = (f32[512]{0:T(512)S(1)}, f32[512,1024]{1,0:T(8,128)S(1)}) fusion(f32[542,1024]{1,0:T(8,128)S(1)} %maximum_convert_fusion, f32[1024]{0:T(1024)S(1)} %bitcast.61, f32[1024]{0:T(1024)S(1)} %bitcast.62, f32[1024]{0:T(1024)S(1)} %bitcast.64, f32[1024]{0:T(1024)S(1)} %bitcast.65, f32[1024]{0:T(1024)S(1)} %bitcast.66, f32[1024]{0:T(1024)S(1)} %bitcast.67, ...), kind=kLoop, calls=%fused_computation.84 | loop fusion | flops 33029632 | bytes 67241984 | tf_op jit(solution)/shard_map/reduce_sum | solution.py:50
  175.8 0.0 copy-start.5
  175.8 0.0 copy-start.6
  175.8 1.3 copy-done.1
  177.1 0.3 multiply_reduce_fusion
  177.4 19.4 %all-gather.8.cloned.1.call-done = bf16[1024,2048]{1,0:T(8,128)(2,1)} async-done(((bf16[1024,256]{1,0:T(8,128)(2,1)}), bf16[1024,2048]{1,0:T(8,128)(2,1)}) %all-gather.8.cloned.1.call-update) | async-done | bytes 4194320 | tf_op jit(solution)/shard_map/all_gather | solution.py:58
  196.8 7.0 %fusion = bf16[1,512,2048]{2,1,0:T(8,128)(2,1)} fusion(bf16[1024,2048]{1,0:T(8,128)(2,1)} %all-gather.8.cloned.1.call-done, f32[512,1024]{1,0:T(8,128)} %copy-done.1, f32[1024]{0:T(1024)S(1)} %copy-done.5, f32[1024]{0:T(1024)S(1)} %copy-done.6, f32[512]{0:T(512)S(1)} %add_rsqrt_fusion, f32[512]{0:T(512)S(1)} %broadcast_multiply_fusion), kind=kOutput, calls=%fused_computation.1 | convolution fusion | flops 2153250816 | bytes 8400896 | tf_op jit(solution)/shard_map/dot_general | solution.py:56
  (9 shorter events, 0.1 us)
Async XLA Ops:
  6.5 145.8 %copy-start = (bf16[1,512,2048]{2,1,0:T(8,128)(2,1)S(1)}, bf16[1,512,2048]{2,1,0:T(8,128)(2,1)}, u32[]{:S(2)}) copy-start(bf16[1,512,2048]{2,1,0:T(8,128)(2,1)} %param.8) | copy-start | bytes 6291460
  6.6 75.5 %all-gather.4.cloned.1.call-start = ((), (), s32[]{:S(2)}) async-start(), calls=%async_computation | async-start | bytes 1114112 | tf_op jit(solution)/shard_map/all_gather | solution.py:12
  8.2 144.2 %all-gather.6.cloned.1.call-start = ((), (), s32[]{:S(2)}) async-start(), calls=%async_computation.1 | async-start | bytes 9437184 | tf_op jit(solution)/shard_map/all_gather | solution.py:33
  83.3 1.2 copy-start.3
  83.3 28.2 %copy-start.2 = (f32[31,1024]{1,0:T(8,128)S(1)}, f32[31,1024]{1,0:T(8,128)}, u32[]{:S(2)}) copy-start(f32[31,1024]{1,0:T(8,128)} %param.11) | copy-start | bytes 380932
  84.4 112.4 %all-gather.8.cloned.1.call-start = ((), (), s32[]{:S(2)}) async-start(), calls=%async_computation.2 | async-start | bytes 4718592 | tf_op jit(solution)/shard_map/all_gather | solution.py:58
  161.1 4.5 %collective-permute-start = (bf16[30,1024]{1,0:T(8,128)(2,1)S(1)}, bf16[30,1024]{1,0:T(8,128)(2,1)S(1)}, u32[]{:S(2)}, u32[]{:S(2)}) collective-permute-start(bf16[30,1024]{1,0:T(8,128)(2,1)S(1)} %slice_bitcast_fusion.2), channel_id=1, source_target_pairs={{0,8},{8,16},{16,24},{24,32},{32,40},{40,48},{48,56},{56,64},{64,7... | collective-permute-start | bytes 184328 | tf_op jit(solution)/shard_map/ppermute | solution.py:19
  164.9 1.0 copy-start.4
  175.7 1.3 copy-start.1
  175.8 21.1 %copy-start.5 = (f32[1024]{0:T(1024)S(1)}, f32[1024]{0:T(1024)}, u32[]{:S(2)}) copy-start(f32[1024]{0:T(1024)} %param.14) | copy-start | bytes 12292
  175.8 21.1 %copy-start.6 = (f32[1024]{0:T(1024)S(1)}, f32[1024]{0:T(1024)}, u32[]{:S(2)}) copy-start(f32[1024]{0:T(1024)} %param.13) | copy-start | bytes 12292
Sparse Core Ops, SparseCore 0:
  9.1 72.8 all-gather.3
  84.6 67.7 all-gather.5
  154.2 42.5 all-gather.7
where the time goes:
time: 211 us; the launch traced here: 210 us
  waiting for transfers between devices  135 us (64%)
  blocking collectives  26.9 us (13%)
  matrix products  15 us (7%)
  other arithmetic  14.3 us (7%)
  between operations  13.3 us (6%)
  starting transfers between devices  3.33 us (2%)
  local copies, waits for them, and re-layouts  2.71 us (1%)
    all_gather x1, waiting for transfers between devices, in_one_piece(): filled = lax.all_gather(both, axis, axis=dim, tiled=True)  73.8 us
    all_gather x1, waiting for transfers between devices, local(): lax.all_gather(stacked, 'dp', axis=2, tiled=True)  40.7 us
    all_gather x1, blocking collectives, local(): whole_output = lax.all_gather(out_weight, 'sp', axis=0, tiled=True)  26.9 us
    all_gather x1, waiting for transfers between devices, local(): lax.all_gather(whole_output, 'dp', axis=1, tiled=True)  19.4 us
    reduce_sum x1, other arithmetic, local(): mean_row = jnp.mean(conv_sum, axis=-1, keepdims=True)  9.83 us
    dot_general x1, matrix products, local(): jnp.einsum('td,kdc->ktc', tokens, lax.all_gather(stacked, 'dp', axis=2, t...  8.07 us
    dot_general x1, matrix products, local(): jnp.dot(swished, lax.all_gather(whole_output, 'dp', axis=1, tiled=True),...  6.97 us
  transfers between devices with their start and end apart: 4, of which 4 were waited for; matrix products, arithmetic and copies ran while one was open for 9% of the time, Pallas kernels for 0%

commit v1 on v0

--- a/solution.py
+++ b/solution.py
@@ -30,7 +30,9 @@
     both_rows = jnp.einsum(
         "td,kdc->ktc",
         tokens,
-        lax.all_gather(stacked, "dp", axis=2, tiled=True),
+        jnp.concatenate(
+            lax.all_to_all(jnp.stack([stacked] * lax.axis_size("dp")), "dp", 0, 0), axis=2
+        ),
         preferred_element_type=jnp.float32,
     )
     value_rows = both_rows[0]

time: 211 us -> 256 us (1.21)
  waiting for transfers between devices: 135 us -> 156 us
  starting transfers between devices: 3.33 us -> 19.5 us
  local copies, waits for them, and re-layouts: 2.71 us -> 7.57 us
    all_to_all x0 -> x1, waiting for transfers between devices: none -> 81.6 us  [local(): lax.all_to_all(jnp.stack([stacked] * lax.axis_size('dp')), 'dp', 0, 0)]
    all_gather x1 -> x0, waiting for transfers between devices: 40.7 us -> none  [local(): lax.all_gather(stacked, 'dp', axis=2, tiled=True)]
    all_gather x1, waiting for transfers between devices: 19.4 us -> 0.03 us  [local(): lax.all_gather(whole_output, 'dp', axis=1, tiled=True)]
    all_to_all x0 -> x1, starting transfers between devices: none -> 16.5 us  [local(): lax.all_to_all(jnp.stack([stacked] * lax.axis_size('dp')), 'dp', 0, 0)]
    another operation x0 -> x1, local copies, waits for them, and re-layouts: none -> 4.86 us  [local(): jnp.stack([stacked] * lax.axis_size('dp'))]
  transfers between devices with their start and end apart: 4 -> 4, of which waited for: 4 -> 3; matrix products, arithmetic and copies ran while one was open for 9% -> 8% of each run, Pallas kernels for 0% -> 0%
where the time goes in v1:
time: 256 us
  waiting for transfers between devices  156 us (61%)
  blocking collectives  28.9 us (11%)
  starting transfers between devices  19.5 us (8%)
  matrix products  15 us (6%)
  between operations  15 us (6%)
  other arithmetic  13.3 us (5%)
  local copies, waits for them, and re-layouts  7.57 us (3%)
    all_to_all x1, waiting for transfers between devices, local(): lax.all_to_all(jnp.stack([stacked] * lax.axis_size('dp')), 'dp', 0, 0)  81.6 us
    all_gather x1, waiting for transfers between devices, in_one_piece(): filled = lax.all_gather(both, axis, axis=dim, tiled=True)  73.8 us
    all_gather x1, blocking collectives, local(): whole_output = lax.all_gather(out_weight, 'sp', axis=0, tiled=True)  28.9 us
    all_to_all x1, starting transfers between devices, local(): lax.all_to_all(jnp.stack([stacked] * lax.axis_size('dp')), 'dp', 0, 0)  16.5 us
    reduce_sum x1, other arithmetic, local(): mean_row = jnp.mean(conv_sum, axis=-1, keepdims=True)  9.83 us
    dot_general x1, matrix products, local(): jnp.einsum('td,kdc->ktc', tokens, jnp.concatenate(lax.all_to_all(jnp.stac...  8.06 us
    dot_general x1, matrix products, local(): jnp.dot(swished, lax.all_gather(whole_output, 'dp', axis=1, tiled=True),...  6.97 us
  transfers between devices with their start and end apart: 4, of which 3 were waited for; matrix products, arithmetic and copies ran while one was open for 8% of the time, Pallas kernels for 0%

profile of v1, /device:TPU:33, one launch (start us, length us, event | category | flops | bytes accessed | tf_op | source)
XLA Modules:
  0.0 255.7 jit_solution(10089651937803572025)
XLA Ops:
  7.4 0.0 copy-start
  7.4 0.0 all-gather.3.cloned.1.call-start
  7.4 1.6 pad_maximum_fusion.1
  9.0 0.1 all-gather.3.cloned.1.call-update
  9.0 73.8 %all-gather.3.cloned.1.call-done = bf16[2048,256]{1,0:T(8,128)(2,1)} async-done(((bf16[128,256]{1,0:T(8,128)(2,1)}), bf16[2048,256]{1,0:T(8,128)(2,1)}) %all-gather.3.cloned.1.call-update) | async-done | bytes 1048592 | tf_op jit(solution)/shard_map/all_gather | solution.py:12
  82.9 1.3 slice_bitcast_fusion.1
  84.1 0.1 pad_maximum_fusion
  84.2 4.9 %stack.11 = bf16[8,2,2048,128]{3,2,1,0:T(8,128)(2,1)} broadcast(bf16[2,2048,128]{2,1,0:T(8,128)(2,1)S(1)} %pad_maximum_fusion), dimensions={1,2,3} | broadcast | bytes 9437184 | tf_op jit(solution)/shard_map/stack | solution.py:34
  89.1 16.5 %all-to-all-start = ((bf16[8,2,2048,128]{3,2,1,0:T(8,128)(2,1)}), bf16[8,2,2048,128]{3,2,1,0:T(8,128)(2,1)}, u32[]{:S(2)}, u32[]{:S(2)}) async-start(bf16[8,2,2048,128]{3,2,1,0:T(8,128)(2,1)} %stack.11), calls=%async_computation | async-start | bytes 16777216 | tf_op jit(solution)/shard_map/all_to_all | solution.py:34
  105.6 0.0 all-gather.5.cloned.1.call-start
  105.6 0.0 copy-done.3
  105.6 28.9 %all_gather.10 = bf16[1024,256]{1,0:T(8,128)(2,1)} all-gather(bf16[64,256]{1,0:T(8,128)(2,1)S(1)} %copy-done.3), channel_id=1, replica_groups=mesh['grp'=2,'sp'=16,'dp'=8] {'sp'}, dimensions={0}, use_global_device_ids=true | all-gather | bytes 557056 | tf_op jit(solution)/shard_map/all_gather | solution.py:57
  134.5 0.1 all-gather.5.cloned.1.call-update
  134.6 0.0 copy-done.2
  134.6 0.1 fusion.48
  134.7 81.6 %all-to-all-done = bf16[8,2,2048,128]{3,2,1,0:T(8,128)(2,1)} async-done(((bf16[8,2,2048,128]{3,2,1,0:T(8,128)(2,1)}), bf16[8,2,2048,128]{3,2,1,0:T(8,128)(2,1)}, u32[]{:S(2)}, u32[]{:S(2)}) %all-to-all-start) | async-done | bytes 8388640 | tf_op jit(solution)/shard_map/all_to_all | solution.py:34
  216.3 0.0 copy-done
  216.3 8.1 %convert_bitcast_fusion = bf16[2,512,1024]{2,1,0:T(8,128)(2,1)S(1)} fusion(bf16[1,512,2048]{2,1,0:T(8,128)(2,1)S(1)} %copy-done, bf16[8,2,2048,128]{3,2,1,0:T(8,128)(2,1)} %all-to-all-done), kind=kOutput, calls=%fused_computation.69 | convolution fusion | flops 4296015872 | bytes 12582912 | tf_op jit(solution)/shard_map/td,kdc->ktc/dot_general | solution.py:30
  224.4 0.6 multiply_convert_fusion
  225.0 3.1 %collective-permute-start = (bf16[30,1024]{1,0:T(8,128)(2,1)S(1)}, bf16[30,1024]{1,0:T(8,128)(2,1)S(1)}, u32[]{:S(2)}, u32[]{:S(2)}) collective-permute-start(bf16[30,1024]{1,0:T(8,128)(2,1)S(1)} %slice_bitcast_fusion.2), channel_id=1, source_target_pairs={{0,8},{8,16},{16,24},{24,32},{32,40},{40,48},{48,56},{56,64},{64,7... | collective-permute-start | bytes 184328 | tf_op jit(solution)/shard_map/ppermute | solution.py:19
  228.1 0.6 fusion.51
  228.7 0.0 copy-start.4
  228.7 0.7 collective-permute-done
  229.4 0.3 maximum_convert_fusion
  229.7 0.0 copy-done.4
  229.7 9.8 %fusion.46 = (f32[512]{0:T(512)S(1)}, f32[512,1024]{1,0:T(8,128)S(1)}) fusion(f32[542,1024]{1,0:T(8,128)S(1)} %maximum_convert_fusion, f32[1024]{0:T(1024)S(1)} %bitcast.70, f32[1024]{0:T(1024)S(1)} %bitcast.71, f32[1024]{0:T(1024)S(1)} %bitcast.73, f32[1024]{0:T(1024)S(1)} %bitcast.74, f32[1024]{0:T(1024)S(1)} %bitcast.75, f32[1024]{0:T(1024)S(1)} %bitcast.76, ...), kind=kLoop, calls=%fused_computation.86 | loop fusion | flops 33029632 | bytes 67241984 | tf_op jit(solution)/shard_map/reduce_sum | solution.py:52
  239.5 0.0 copy-start.5
  239.5 0.0 copy-start.6
  239.6 1.3 copy-done.1
  240.9 0.3 multiply_reduce_fusion
  241.2 0.0 all-gather.5.cloned.1.call-done
  241.3 7.0 %fusion.3 = bf16[1,512,2048]{2,1,0:T(8,128)(2,1)} fusion(bf16[1024,2048]{1,0:T(8,128)(2,1)} %all-gather.5.cloned.1.call-done, f32[512,1024]{1,0:T(8,128)} %copy-done.1, f32[1024]{0:T(1024)S(1)} %copy-done.5, f32[1024]{0:T(1024)S(1)} %copy-done.6, f32[512]{0:T(512)S(1)} %add_rsqrt_fusion, f32[512]{0:T(512)S(1)} %broadcast_multiply_fusion), kind=kOutput, calls=%fused_computation.4 | convolution fusion | flops 2153250816 | bytes 8400896 | tf_op jit(solution)/shard_map/dot_general | solution.py:58
  (9 shorter events, 0.1 us)
Async XLA Ops:
  7.4 208.9 %copy-start = (bf16[1,512,2048]{2,1,0:T(8,128)(2,1)S(1)}, bf16[1,512,2048]{2,1,0:T(8,128)(2,1)}, u32[]{:S(2)}) copy-start(bf16[1,512,2048]{2,1,0:T(8,128)(2,1)} %param.8) | copy-start | bytes 6291460
  7.4 75.5 %all-gather.3.cloned.1.call-start = ((), (), s32[]{:S(2)}) async-start(), calls=%async_computation.1 | async-start | bytes 1114112 | tf_op jit(solution)/shard_map/all_gather | solution.py:12
  89.1 16.5 %copy-start.3 = (bf16[64,256]{1,0:T(8,128)(2,1)S(1)}, bf16[64,256]{1,0:T(8,128)(2,1)}, u32[]{:S(2)}) copy-start(bf16[64,256]{1,0:T(8,128)(2,1)} %param.15) | copy-start | bytes 98308
  89.1 45.5 %copy-start.2 = (f32[31,1024]{1,0:T(8,128)S(1)}, f32[31,1024]{1,0:T(8,128)}, u32[]{:S(2)}) copy-start(f32[31,1024]{1,0:T(8,128)} %param.11) | copy-start | bytes 380932
  89.1 127.2 %all-to-all-start = ((bf16[8,2,2048,128]{3,2,1,0:T(8,128)(2,1)}), bf16[8,2,2048,128]{3,2,1,0:T(8,128)(2,1)}, u32[]{:S(2)}, u32[]{:S(2)}) async-start(bf16[8,2,2048,128]{3,2,1,0:T(8,128)(2,1)} %stack.11), calls=%async_computation | async-start | bytes 16777216 | tf_op jit(solution)/shard_map/all_to_all | solution.py:34
  105.6 135.7 %all-gather.5.cloned.1.call-start = ((), (), s32[]{:S(2)}) async-start(), calls=%async_computation.2 | async-start | bytes 4718592 | tf_op jit(solution)/shard_map/all_gather | solution.py:60
  225.0 4.4 %collective-permute-start = (bf16[30,1024]{1,0:T(8,128)(2,1)S(1)}, bf16[30,1024]{1,0:T(8,128)(2,1)S(1)}, u32[]{:S(2)}, u32[]{:S(2)}) collective-permute-start(bf16[30,1024]{1,0:T(8,128)(2,1)S(1)} %slice_bitcast_fusion.2), channel_id=1, source_target_pairs={{0,8},{8,16},{16,24},{24,32},{32,40},{40,48},{48,56},{56,64},{64,7... | collective-permute-start | bytes 184328 | tf_op jit(solution)/shard_map/ppermute | solution.py:19
  228.7 1.0 copy-start.4
  239.5 1.3 copy-start.1
  239.5 1.7 copy-start.5
  239.5 1.7 copy-start.6
Sparse Core Ops, SparseCore 0:
  10.0 72.8 all-gather.2
Sparse Core Ops, SparseCore 1:
  134.6 68.1 all-gather.4
